TPU v7x, 32 devices: a whole 2x2x4 slice. The times are simulated.
32 devices in a mesh: fs: 8 (over z, y), tp: 4 (over x, core).
Axes of the slice: x: 2, y: 2, z: 4, core: 2. Of those that a mesh axis runs over, the one named last changes fastest.
Arguments:
- tokens: bfloat16 [640, 3072], P('tp'), may hold values from -6 to 6
- gain_first: float32 [3072], replicated, may hold values from 0.1 to 1.9
- gain_second: float32 [3072], replicated, may hold values from 0.1 to 1.9
- gate_first: float32 [3072, 8192], P('fs', 'tp'), may hold values from -0.109375 to 0.109375
- up_first: float32 [3072, 8192], P('fs', 'tp'), may hold values from -0.109375 to 0.109375
- down_first: float32 [8192, 3072], P('fs', 'tp'), may hold values from -0.09375 to 0.09375
- gate_second: float32 [3072, 8192], P('fs', 'tp'), may hold values from -0.109375 to 0.109375
- up_second: float32 [3072, 8192], P('fs', 'tp'), may hold values from -0.109375 to 0.109375
- down_second: float32 [8192, 3072], P('fs', 'tp'), may hold values from -0.09375 to 0.09375
Outputs:
- result_rows: bfloat16 [640, 3072], P('tp')
- serve_gate_first: bfloat16 [3072, 8192], P(None, 'fs')
- serve_up_first: bfloat16 [3072, 8192], P(None, 'fs')
- serve_down_first: bfloat16 [8192, 3072], P('fs')
- serve_gate_second: bfloat16 [3072, 8192], P(None, 'fs')
- serve_up_second: bfloat16 [3072, 8192], P(None, 'fs')
- serve_down_second: bfloat16 [8192, 3072], P('fs')
All inputs are finite; a program needn't handle non-finite values.
Results may differ from a plain program's by a relative error of at most 0.011.
Values may be sent and summed in bfloat16 or wider, within the bound.
A program may use at most 192 MiB of HBM per device.

v0:
```python
import jax
import jax.numpy as jnp
from jax import lax
from jax.sharding import PartitionSpec as P


def plain_norm(values):
    values = values.astype(jnp.float32)
    center = jnp.mean(values, axis=-1, keepdims=True)
    spread = jnp.mean(jnp.square(values - center), axis=-1, keepdims=True)
    return (values - center) * lax.rsqrt(spread + 1e-05)


def sum_over_hidden(partial_value):
    pieces = lax.all_to_all(
        partial_value.astype(jnp.bfloat16), "fs", split_axis=1, concat_axis=0, tiled=True
    )
    rows = partial_value.shape[0]
    pieces = pieces.reshape(-1, rows, pieces.shape[1]).astype(jnp.float32)
    summed = jnp.sum(pieces, axis=0).astype(jnp.bfloat16)
    return lax.all_gather(summed, "fs", axis=1, tiled=True).astype(jnp.float32)


def regroup(folded):
    spread = lax.all_to_all(folded, "tp", split_axis=0, concat_axis=1, tiled=True)
    parts = lax.axis_size("fs")
    rows = spread.shape[0]
    owned = lax.all_to_all(spread, "fs", split_axis=1, concat_axis=0, tiled=True)
    owned = owned.reshape(parts, rows, owned.shape[1])
    whole = lax.all_gather(owned, "tp", axis=1, tiled=True)
    return whole.reshape(-1, whole.shape[2])


def half_step(normed, scales, w_gate, w_rising, w_down):
    gate_part = jnp.dot(normed, w_gate, preferred_element_type=jnp.float32)
    rising = jnp.dot(normed, w_rising, preferred_element_type=jnp.float32)
    hidden = (jax.nn.silu(gate_part) * rising).astype(jnp.bfloat16)
    partial_value = jnp.dot(hidden, w_down, preferred_element_type=jnp.float32)
    block = sum_over_hidden(partial_value)
    mixed = 1.6817928 * scales[None, :] * normed.astype(jnp.float32) + 0.5 * block
    return plain_norm(mixed).astype(jnp.bfloat16)


def on_device(
    tokens,
    gain_first,
    gain_second,
    gate_first,
    up_first,
    down_first,
    gate_second,
    up_second,
    down_second,
):
    row_count = gate_first.shape[0]
    offset = lax.axis_index("fs") * row_count

    def fold_gain(weight, scales):
        picked = lax.dynamic_slice_in_dim(scales, offset, row_count, 0)
        return (picked[:, None] * weight).astype(jnp.bfloat16)

    serve_gate_first = regroup(fold_gain(gate_first, gain_first))
    serve_up_first = regroup(fold_gain(up_first, gain_first))
    serve_down_first = lax.all_gather(down_first.astype(jnp.bfloat16), "tp", axis=1, tiled=True)
    serve_gate_second = regroup(fold_gain(gate_second, gain_second))
    serve_up_second = regroup(fold_gain(up_second, gain_second))
    serve_down_second = lax.all_gather(down_second.astype(jnp.bfloat16), "tp", axis=1, tiled=True)
    normed_zero = plain_norm(tokens).astype(jnp.bfloat16)
    normed_one = half_step(
        normed_zero, gain_first, serve_gate_first, serve_up_first, serve_down_first
    )
    result_rows = half_step(
        normed_one, gain_second, serve_gate_second, serve_up_second, serve_down_second
    )
    return (
        result_rows,
        serve_gate_first,
        serve_up_first,
        serve_down_first,
        serve_gate_second,
        serve_up_second,
        serve_down_second,
    )


def solution(mesh):
    placed = (
        P("tp", None),
        P(),
        P(),
        P("fs", "tp"),
        P("fs", "tp"),
        P("fs", "tp"),
        P("fs", "tp"),
        P("fs", "tp"),
        P("fs", "tp"),
    )
    return jax.shard_map(
        on_device,
        mesh=mesh,
        in_specs=placed,
        out_specs=(
            P("tp", None),
            P(None, "fs"),
            P(None, "fs"),
            P("fs", None),
            P(None, "fs"),
            P(None, "fs"),
            P("fs", None),
        ),
        check_vma=False,
    )
```

profile of v0, /device:TPU:0, one launch (start us, length us, event | category | flops | bytes accessed | tf_op | source)
XLA Modules:
  0.0 523.0 jit_solution(2696292961990616382)
XLA Ops:
  8.0 3.7 multiply_convert_fusion.3
  11.7 24.1 %all_to_all.154 = bf16[4,96,2048]{2,1,0:T(8,128)(2,1)S(1)} all-to-all(bf16[4,96,2048]{2,1,0:T(8,128)(2,1)S(1)} %bitcast.44), channel_id=1, replica_groups=mesh['fs'=8,'tp'=4] {'tp'}, dimensions={0} | all-to-all | bytes 3145728 | tf_op jit(solution)/shard_map/all_to_all | solution.py:25
  37.0 1.8 all_to_all.119
  38.9 2.3 copy.29
  41.2 42.3 %all_to_all.155 = bf16[96,8,1024]{2,0,1:T(8,128)(2,1)S(1)} all-to-all(bf16[96,8,1024]{2,0,1:T(8,128)(2,1)S(1)} %copy.29), channel_id=1, replica_groups=mesh['fs'=8,'tp'=4] {'fs'}, dimensions={1} | all-to-all | bytes 3145728 | tf_op jit(solution)/shard_map/all_to_all | solution.py:28
  83.5 2.0 copy.30
  85.6 36.1 %all_to_all.156 = bf16[4,96,2048]{2,1,0:T(8,128)(2,1)S(1)} all-to-all(bf16[4,96,2048]{2,1,0:T(8,128)(2,1)S(1)} %bitcast.42), channel_id=1, replica_groups=mesh['fs'=8,'tp'=4] {'tp'}, dimensions={0} | all-to-all | bytes 3145728 | tf_op jit(solution)/shard_map/all_to_all | solution.py:25
  124.2 39.1 %all_to_all.157 = bf16[96,8,1024]{2,0,1:T(8,128)(2,1)S(1)} all-to-all(bf16[96,8,1024]{2,0,1:T(8,128)(2,1)S(1)} %copy.33), channel_id=1, replica_groups=mesh['fs'=8,'tp'=4] {'fs'}, dimensions={1} | all-to-all | bytes 3145728 | tf_op jit(solution)/shard_map/all_to_all | solution.py:28
  163.3 2.0 copy.34
  166.8 3.9 multiply_convert_fusion.1
  170.7 39.8 %all_to_all.158 = bf16[4,96,2048]{2,1,0:T(8,128)(2,1)S(1)} all-to-all(bf16[4,96,2048]{2,1,0:T(8,128)(2,1)S(1)} %bitcast.45), channel_id=1, replica_groups=mesh['fs'=8,'tp'=4] {'tp'}, dimensions={0} | all-to-all | bytes 3145728 | tf_op jit(solution)/shard_map/all_to_all | solution.py:25
  211.7 1.8 all_to_all.133
  213.6 2.3 copy.38
  215.8 51.1 %all_to_all.159 = bf16[96,8,1024]{2,0,1:T(8,128)(2,1)S(1)} all-to-all(bf16[96,8,1024]{2,0,1:T(8,128)(2,1)S(1)} %copy.38), channel_id=1, replica_groups=mesh['fs'=8,'tp'=4] {'fs'}, dimensions={1} | all-to-all | bytes 3145728 | tf_op jit(solution)/shard_map/all_to_all | solution.py:28
  266.9 2.0 copy.39
  269.0 26.1 %all_to_all.160 = bf16[4,96,2048]{2,1,0:T(8,128)(2,1)S(1)} all-to-all(bf16[4,96,2048]{2,1,0:T(8,128)(2,1)S(1)} %bitcast.43), channel_id=1, replica_groups=mesh['fs'=8,'tp'=4] {'tp'}, dimensions={0} | all-to-all | bytes 3145728 | tf_op jit(solution)/shard_map/all_to_all | solution.py:25
  297.6 39.2 %all_to_all.161 = bf16[96,8,1024]{2,0,1:T(8,128)(2,1)S(1)} all-to-all(bf16[96,8,1024]{2,0,1:T(8,128)(2,1)S(1)} %copy.42), channel_id=1, replica_groups=mesh['fs'=8,'tp'=4] {'fs'}, dimensions={1} | all-to-all | bytes 3145728 | tf_op jit(solution)/shard_map/all_to_all | solution.py:28
  336.8 2.0 copy.43
  342.0 9.7 %copy.31 = bf16[8,384,1024]{2,1,0:T(8,128)(2,1)} copy(bf16[8,384,1024]{2,0,1:T(8,128)(2,1)} %all-gather.7.cloned.1.call-done) | data formatting | bytes 12582912 | tf_op jit(solution)/shard_map/all_gather | solution.py:30
  351.7 9.2 %copy.35 = bf16[8,384,1024]{2,1,0:T(8,128)(2,1)} copy(bf16[8,384,1024]{2,0,1:T(8,128)(2,1)} %all-gather.9.cloned.1.call-done) | data formatting | bytes 12582912 | tf_op jit(solution)/shard_map/all_gather | solution.py:30
  362.3 7.0 %convolution_convert_fusion.1 = bf16[160,3072]{1,0:T(8,128)(2,1)S(1)} fusion(bf16[1024,3072]{1,0:T(8,128)(2,1)} %all-gather.11.cloned.1.call-done, bf16[3072,1024]{1,0:T(8,128)(2,1)} %bitcast.38, f32[160,1024]{1,0:T(8,128)S(1)} %fusion.14, bf16[160,3072]{1,0:T(8,128)(2,1)S(1)} %copy-done.1, f32[160]{0:T(256)S(1)} %add_rsqrt_fusion.2, ...), kind=kOutput, calls=%fused_computation.1 | convolution fusion | flops 2016706560 | bytes 15205632 | tf_op jit(solution)/shard_map/dot_general | solution.py:38
  370.3 3.8 all-to-all-start.4
  374.1 9.1 %copy.40 = bf16[8,384,1024]{2,1,0:T(8,128)(2,1)} copy(bf16[8,384,1024]{2,0,1:T(8,128)(2,1)} %all-gather.13.cloned.1.call-done) | data formatting | bytes 12582912 | tf_op jit(solution)/shard_map/all_gather | solution.py:30
  383.7 9.0 %copy.44 = bf16[8,384,1024]{2,1,0:T(8,128)(2,1)} copy(bf16[8,384,1024]{2,0,1:T(8,128)(2,1)} %all-gather.15.cloned.1.call-done) | data formatting | bytes 12582912 | tf_op jit(solution)/shard_map/all_gather | solution.py:30
  392.7 5.5 %all-to-all-done.4 = bf16[160,8,384]{2,0,1:T(8,128)(2,1)S(1)} async-done(((bf16[160,8,384]{2,0,1:T(8,128)(2,1)}), bf16[160,8,384]{2,0,1:T(8,128)(2,1)S(1)}, u32[]{:S(2)}, u32[]{:S(2)}) %all-to-all-start.4) | async-done | bytes 983072 | tf_op jit(solution)/shard_map/all_to_all | solution.py:15
  398.3 33.7 %all_gather.27 = bf16[160,3072]{1,0:T(8,128)(2,1)S(1)} all-gather(bf16[160,384]{1,0:T(8,128)(2,1)S(1)} %reduce_sum.80), channel_id=1, replica_groups=mesh['fs'=8,'tp'=4] {'fs'}, dimensions={1}, use_global_device_ids=true | all-gather | bytes 1105920 | tf_op jit(solution)/shard_map/all_gather | solution.py:21
  436.0 6.9 %convolution_convert_fusion = bf16[160,3072]{1,0:T(8,128)(2,1)S(1)} fusion(bf16[1024,3072]{1,0:T(8,128)(2,1)} %all-gather.17.cloned.1.call-done, bf16[160,3072]{1,0:T(8,128)(2,1)S(1)} %multiply_convert_fusion.5, bf16[3072,1024]{1,0:T(8,128)(2,1)} %bitcast.40, f32[160,1024]{1,0:T(8,128)S(1)} %fusion.16), kind=kOutput, calls=%fused_computation | convolution fusion | flops 2014740480 | bytes 15204352 | tf_op jit(solution)/shard_map/dot_general | solution.py:38
  444.0 3.6 all-to-all-start.9
  447.6 23.0 %all-to-all-done.9 = bf16[160,8,384]{2,0,1:T(8,128)(2,1)S(1)} async-done(((bf16[160,8,384]{2,0,1:T(8,128)(2,1)}), bf16[160,8,384]{2,0,1:T(8,128)(2,1)S(1)}, u32[]{:S(2)}, u32[]{:S(2)}) %all-to-all-start.9) | async-done | bytes 983072 | tf_op jit(solution)/shard_map/all_to_all | solution.py:15
  470.6 33.6 %all_gather.31 = bf16[160,3072]{1,0:T(8,128)(2,1)S(1)} all-gather(bf16[160,384]{1,0:T(8,128)(2,1)S(1)} %reduce_sum.83), channel_id=1, replica_groups=mesh['fs'=8,'tp'=4] {'fs'}, dimensions={1}, use_global_device_ids=true | all-gather | bytes 1105920 | tf_op jit(solution)/shard_map/all_gather | solution.py:21
  506.9 6.1 %copy.54 = bf16[1024,3072]{1,0:T(8,128)(2,1)} copy(bf16[1024,3072]{1,0:T(8,128)(2,1)} %all-gather.11.cloned.1.call-done) | data formatting | bytes 12582912
  513.0 2.7 copy.55
  (71 shorter events, 23.9 us)
Async XLA Ops:
  7.2 334.9 %all-gather.7.cloned.1.call-start = ((), (), s32[]{:S(2)}) async-start(), calls=%async_computation.10 | async-start | bytes 7864320 | tf_op jit(solution)/shard_map/all_gather | solution.py:30
  85.5 266.2 %all-gather.9.cloned.1.call-start = ((), (), s32[]{:S(2)}) async-start(), calls=%async_computation.11 | async-start | bytes 7864320 | tf_op jit(solution)/shard_map/all_gather | solution.py:30
  163.3 2.1 copy-start.3
  165.3 1.4 copy-start.6
  165.3 196.9 %all-gather.11.cloned.1.call-start = ((), (), s32[]{:S(2)}) async-start(), calls=%async_computation.12 | async-start | bytes 7864320 | tf_op jit(solution)/shard_map/all_gather | solution.py:64
  166.7 207.4 %all-gather.13.cloned.1.call-start = ((), (), s32[]{:S(2)}) async-start(), calls=%async_computation.13 | async-start | bytes 7864320 | tf_op jit(solution)/shard_map/all_gather | solution.py:30
  269.0 114.7 %all-gather.15.cloned.1.call-start = ((), (), s32[]{:S(2)}) async-start(), calls=%async_computation.14 | async-start | bytes 7864320 | tf_op jit(solution)/shard_map/all_gather | solution.py:30
  336.8 2.1 copy-start.4
  338.8 97.2 %all-gather.17.cloned.1.call-start = ((), (), s32[]{:S(2)}) async-start(), calls=%async_computation.15 | async-start | bytes 7864320 | tf_op jit(solution)/shard_map/all_gather | solution.py:67
  340.2 1.2 copy-start.1
  351.7 9.2 %copy-start.2 = (bf16[8,384,1024]{2,1,0:T(8,128)(2,1)S(1)}, bf16[8,384,1024]{2,1,0:T(8,128)(2,1)}, u32[]{:S(2)}) copy-start(bf16[8,384,1024]{2,1,0:T(8,128)(2,1)} %copy.31) | copy-start | bytes 18874372
  369.3 4.8 copy-start.5
  370.3 27.8 %all-to-all-start.4 = ((bf16[160,8,384]{2,0,1:T(8,128)(2,1)}), bf16[160,8,384]{2,0,1:T(8,128)(2,1)S(1)}, u32[]{:S(2)}, u32[]{:S(2)}) async-start(bf16[160,8,384]{2,0,1:T(8,128)(2,1)} %bitcast.31), calls=%async_computation.4 | async-start | bytes 1966080 | tf_op jit(solution)/shard_map/all_to_all | solution.py:15
  432.0 2.8 copy-start
  444.0 26.5 %all-to-all-start.9 = ((bf16[160,8,384]{2,0,1:T(8,128)(2,1)}), bf16[160,8,384]{2,0,1:T(8,128)(2,1)S(1)}, u32[]{:S(2)}, u32[]{:S(2)}) async-start(bf16[160,8,384]{2,0,1:T(8,128)(2,1)} %bitcast.30), calls=%async_computation.9 | async-start | bytes 1966080 | tf_op jit(solution)/shard_map/all_to_all | solution.py:15
  505.4 7.6 %slice-start = ((s8[6291456]{0:T(1024)(128)(4,1)}), s8[4194304]{0:T(1024)(128)(4,1)S(1)}, s32[]{:S(2)}) async-start(s8[6291456]{0:T(1024)(128)(4,1)} %bitcast.34), calls=%async_computation.16 | async-start | bytes 8388608
  506.9 6.1 %slice-start.1 = ((s8[6291456]{0:T(1024)(128)(4,1)}), s8[2097152]{0:T(1024)(128)(4,1)S(1)}, s32[]{:S(2)}) async-start(s8[6291456]{0:T(1024)(128)(4,1)} %bitcast.34), calls=%async_computation.17 | async-start | bytes 4194304
Sparse Core Ops, SparseCore 0:
  85.6 57.7 all-gather.6
  165.4 61.2 all-gather.8
  228.8 46.1 all-gather.10
  276.5 50.4 all-gather.12
  338.9 44.6 all-gather.14
  385.7 46.3 all-gather.16
where the time goes:
time: 532 us; the launch traced here: 523 us
  blocking collectives  365 us (69%)
  local copies, waits for them, and re-layouts  74 us (14%)
  waiting for transfers between devices  29.1 us (5%)
  matrix products  16.4 us (3%)
  other arithmetic  16.1 us (3%)
  between operations  14.8 us (3%)
  starting transfers between devices  7.57 us (1%)
    all_to_all x4, blocking collectives, regroup(): lax.all_to_all(spread, 'fs', split_axis=1, concat_axis=0, tiled=True)  172 us
    all_to_all x4, blocking collectives, regroup(): lax.all_to_all(folded, 'tp', split_axis=0, concat_axis=1, tiled=True)  126 us
    all_gather x2, blocking collectives, sum_over_hidden(): return lax.all_gather(summed, 'fs', axis=1, tiled=True).astype(jnp.float32)  67.3 us
    all_gather x4, local copies, waits for them, and re-layouts, regroup(): whole = lax.all_gather(owned, 'tp', axis=1, tiled=True)  36.9 us
    all_to_all x2, waiting for transfers between devices, sum_over_hidden(): lax.all_to_all(partial_value.astype(jnp.bfloat16), 'fs', split_axis=1, co...  28.4 us
    all_to_all x12, local copies, waits for them, and re-layouts, regroup(): lax.all_to_all(spread, 'fs', split_axis=1, concat_axis=0, tiled=True)  18.8 us
    dot_general x2, matrix products, half_step(): partial_value = jnp.dot(hidden, w_down, preferred_element_type=jnp.float32)  13.9 us
  transfers between devices with their start and end apart: 8, of which 3 were waited for; matrix products, arithmetic and copies ran while one was open for 14% of the time, Pallas kernels for 0%

commit v1 on v0

--- a/solution.py
+++ b/solution.py
@@ -18,7 +18,9 @@
     rows = partial_value.shape[0]
     pieces = pieces.reshape(-1, rows, pieces.shape[1]).astype(jnp.float32)
     summed = jnp.sum(pieces, axis=0).astype(jnp.bfloat16)
-    return lax.all_gather(summed, "fs", axis=1, tiled=True).astype(jnp.float32)
+    return jnp.concatenate(
+        lax.all_to_all(jnp.stack([summed] * lax.axis_size("fs")), "fs", 0, 0), axis=1
+    ).astype(jnp.float32)
 
 
 def regroup(folded):

time: 532 us -> 526 us (0.989)
  blocking collectives: 365 us -> 355 us
    all_gather x2 -> x0, blocking collectives: 67.3 us -> none  [sum_over_hidden(): return lax.all_gather(summed, 'fs', axis=1, tiled=True).astype(jnp.float32)]
    all_to_all x0 -> x2, blocking collectives: none -> 57.3 us  [sum_over_hidden(): lax.all_to_all(partial_value.astype(jnp.bfloat16), 'fs', split_axis=1, co...]
where the time goes in v1:
time: 526 us; the launch traced here: 516 us
  blocking collectives  355 us (67%)
  local copies, waits for them, and re-layouts  73.8 us (14%)
  waiting for transfers between devices  32.3 us (6%)
  matrix products  16.8 us (3%)
  other arithmetic  15.7 us (3%)
  between operations  14.9 us (3%)
  starting transfers between devices  7.54 us (1%)
    all_to_all x4, blocking collectives, regroup(): lax.all_to_all(spread, 'fs', split_axis=1, concat_axis=0, tiled=True)  172 us
    all_to_all x4, blocking collectives, regroup(): lax.all_to_all(folded, 'tp', split_axis=0, concat_axis=1, tiled=True)  126 us
    all_to_all x2, blocking collectives, sum_over_hidden(): lax.all_to_all(partial_value.astype(jnp.bfloat16), 'fs', split_axis=1, co...  57.3 us
    all_gather x4, local copies, waits for them, and re-layouts, regroup(): whole = lax.all_gather(owned, 'tp', axis=1, tiled=True)  36.9 us
    all_to_all x2, waiting for transfers between devices, sum_over_hidden(): lax.all_to_all(jnp.stack([summed] * lax.axis_size('fs')), 'fs', 0, 0)  30.1 us
    all_to_all x12, local copies, waits for them, and re-layouts, regroup(): lax.all_to_all(spread, 'fs', split_axis=1, concat_axis=0, tiled=True)  18.8 us
    dot_general x2, matrix products, half_step(): partial_value = jnp.dot(hidden, w_down, preferred_element_type=jnp.float32)  14.2 us
  transfers between devices with their start and end apart: 8, of which 3 were waited for; matrix products, arithmetic and copies ran while one was open for 14% of the time, Pallas kernels for 0%

profile of v1, /device:TPU:0, one launch (start us, length us, event | category | flops | bytes accessed | tf_op | source)
XLA Modules:
  0.0 516.4 jit_solution(6241368712151512550)
XLA Ops:
  8.0 3.7 multiply_convert_fusion.3
  11.7 24.1 %all_to_all.164 = bf16[4,96,2048]{2,1,0:T(8,128)(2,1)S(1)} all-to-all(bf16[4,96,2048]{2,1,0:T(8,128)(2,1)S(1)} %bitcast.62), channel_id=1, replica_groups=mesh['fs'=8,'tp'=4] {'tp'}, dimensions={0} | all-to-all | bytes 3145728 | tf_op jit(solution)/shard_map/all_to_all | solution.py:27
  37.0 1.8 all_to_all.125
  38.9 2.3 copy.47
  41.2 42.3 %all_to_all.165 = bf16[96,8,1024]{2,0,1:T(8,128)(2,1)S(1)} all-to-all(bf16[96,8,1024]{2,0,1:T(8,128)(2,1)S(1)} %copy.47), channel_id=1, replica_groups=mesh['fs'=8,'tp'=4] {'fs'}, dimensions={1} | all-to-all | bytes 3145728 | tf_op jit(solution)/shard_map/all_to_all | solution.py:30
  83.5 2.0 copy.48
  85.6 36.1 %all_to_all.166 = bf16[4,96,2048]{2,1,0:T(8,128)(2,1)S(1)} all-to-all(bf16[4,96,2048]{2,1,0:T(8,128)(2,1)S(1)} %bitcast.60), channel_id=1, replica_groups=mesh['fs'=8,'tp'=4] {'tp'}, dimensions={0} | all-to-all | bytes 3145728 | tf_op jit(solution)/shard_map/all_to_all | solution.py:27
  124.2 39.1 %all_to_all.167 = bf16[96,8,1024]{2,0,1:T(8,128)(2,1)S(1)} all-to-all(bf16[96,8,1024]{2,0,1:T(8,128)(2,1)S(1)} %copy.51), channel_id=1, replica_groups=mesh['fs'=8,'tp'=4] {'fs'}, dimensions={1} | all-to-all | bytes 3145728 | tf_op jit(solution)/shard_map/all_to_all | solution.py:30
  163.3 2.0 copy.52
  166.8 3.9 multiply_convert_fusion.1
  170.7 39.8 %all_to_all.168 = bf16[4,96,2048]{2,1,0:T(8,128)(2,1)S(1)} all-to-all(bf16[4,96,2048]{2,1,0:T(8,128)(2,1)S(1)} %bitcast.63), channel_id=1, replica_groups=mesh['fs'=8,'tp'=4] {'tp'}, dimensions={0} | all-to-all | bytes 3145728 | tf_op jit(solution)/shard_map/all_to_all | solution.py:27
  213.6 2.3 copy.57
  215.8 51.2 %all_to_all.169 = bf16[96,8,1024]{2,0,1:T(8,128)(2,1)S(1)} all-to-all(bf16[96,8,1024]{2,0,1:T(8,128)(2,1)S(1)} %copy.57), channel_id=1, replica_groups=mesh['fs'=8,'tp'=4] {'fs'}, dimensions={1} | all-to-all | bytes 3145728 | tf_op jit(solution)/shard_map/all_to_all | solution.py:30
  267.1 2.0 copy.58
  269.2 26.4 %all_to_all.170 = bf16[4,96,2048]{2,1,0:T(8,128)(2,1)S(1)} all-to-all(bf16[4,96,2048]{2,1,0:T(8,128)(2,1)S(1)} %bitcast.61), channel_id=1, replica_groups=mesh['fs'=8,'tp'=4] {'tp'}, dimensions={0} | all-to-all | bytes 3145728 | tf_op jit(solution)/shard_map/all_to_all | solution.py:27
  298.1 39.1 %all_to_all.171 = bf16[96,8,1024]{2,0,1:T(8,128)(2,1)S(1)} all-to-all(bf16[96,8,1024]{2,0,1:T(8,128)(2,1)S(1)} %copy.61), channel_id=1, replica_groups=mesh['fs'=8,'tp'=4] {'fs'}, dimensions={1} | all-to-all | bytes 3145728 | tf_op jit(solution)/shard_map/all_to_all | solution.py:30
  337.2 2.0 copy.62
  342.4 9.7 %copy.49 = bf16[8,384,1024]{2,1,0:T(8,128)(2,1)} copy(bf16[8,384,1024]{2,0,1:T(8,128)(2,1)} %all-gather.7.cloned.1.call-done) | data formatting | bytes 12582912 | tf_op jit(solution)/shard_map/all_gather | solution.py:32
  352.2 9.2 %copy.53 = bf16[8,384,1024]{2,1,0:T(8,128)(2,1)} copy(bf16[8,384,1024]{2,0,1:T(8,128)(2,1)} %all-gather.9.cloned.1.call-done) | data formatting | bytes 12582912 | tf_op jit(solution)/shard_map/all_gather | solution.py:32
  362.7 7.1 %convolution_convert_fusion.1 = bf16[160,3072]{1,0:T(8,128)(2,1)S(1)} fusion(bf16[1024,3072]{1,0:T(8,128)(2,1)} %all-gather.11.cloned.1.call-done, bf16[3072,1024]{1,0:T(8,128)(2,1)} %bitcast.56, f32[160,1024]{1,0:T(8,128)S(1)} %fusion.14, bf16[160,3072]{1,0:T(8,128)(2,1)S(1)} %copy-done, f32[160]{0:T(256)S(1)} %add_rsqrt_fusion.2, ...), kind=kOutput, calls=%fused_computation.1 | convolution fusion | flops 2016706560 | bytes 15205632 | tf_op jit(solution)/shard_map/dot_general | solution.py:40
  369.9 27.1 %all_to_all.172 = bf16[160,8,384]{2,0,1:T(8,128)(2,1)S(1)} all-to-all(bf16[160,8,384]{2,0,1:T(8,128)(2,1)S(1)} %bitcast.72), channel_id=1, replica_groups=mesh['fs'=8,'tp'=4] {'fs'}, dimensions={1} | all-to-all | bytes 1966080 | tf_op jit(solution)/shard_map/all_to_all | solution.py:15
  398.2 3.7 all-to-all-start.5
  402.0 9.0 %copy.59 = bf16[8,384,1024]{2,1,0:T(8,128)(2,1)} copy(bf16[8,384,1024]{2,0,1:T(8,128)(2,1)} %all-gather.13.cloned.1.call-done) | data formatting | bytes 12582912 | tf_op jit(solution)/shard_map/all_gather | solution.py:32
  411.0 9.0 %copy.63 = bf16[8,384,1024]{2,1,0:T(8,128)(2,1)} copy(bf16[8,384,1024]{2,0,1:T(8,128)(2,1)} %all-gather.15.cloned.1.call-done) | data formatting | bytes 12582912 | tf_op jit(solution)/shard_map/all_gather | solution.py:32
  420.0 5.9 %all-to-all-done.5 = bf16[8,160,384]{2,1,0:T(8,128)(2,1)S(1)} async-done(((bf16[8,160,384]{2,1,0:T(8,128)(2,1)}), bf16[8,160,384]{2,1,0:T(8,128)(2,1)S(1)}, u32[]{:S(2)}, u32[]{:S(2)}) %all-to-all-start.5) | async-done | bytes 983072 | tf_op jit(solution)/shard_map/all_to_all | solution.py:22
  430.2 2.0 all-gather.17.cloned.1.call-done
  432.2 7.2 %convolution_convert_fusion = bf16[160,3072]{1,0:T(8,128)(2,1)S(1)} fusion(bf16[1024,3072]{1,0:T(8,128)(2,1)} %all-gather.17.cloned.1.call-done, bf16[160,3072]{1,0:T(8,128)(2,1)S(1)} %multiply_convert_fusion.5, bf16[3072,1024]{1,0:T(8,128)(2,1)} %bitcast.58, f32[160,1024]{1,0:T(8,128)S(1)} %fusion.16), kind=kOutput, calls=%fused_computation | convolution fusion | flops 2014740480 | bytes 15204352 | tf_op jit(solution)/shard_map/dot_general | solution.py:40
  439.5 30.2 %all_to_all.173 = bf16[160,8,384]{2,0,1:T(8,128)(2,1)S(1)} all-to-all(bf16[160,8,384]{2,0,1:T(8,128)(2,1)S(1)} %bitcast.73), channel_id=1, replica_groups=mesh['fs'=8,'tp'=4] {'fs'}, dimensions={1} | all-to-all | bytes 1966080 | tf_op jit(solution)/shard_map/all_to_all | solution.py:15
  470.8 3.6 all-to-all-start.11
  474.4 24.2 %all-to-all-done.11 = bf16[8,160,384]{2,1,0:T(8,128)(2,1)S(1)} async-done(((bf16[8,160,384]{2,1,0:T(8,128)(2,1)}), bf16[8,160,384]{2,1,0:T(8,128)(2,1)S(1)}, u32[]{:S(2)}, u32[]{:S(2)}) %all-to-all-start.11) | async-done | bytes 983072 | tf_op jit(solution)/shard_map/all_to_all | solution.py:22
  501.8 3.2 copy.76
  506.4 2.7 copy.77
  (85 shorter events, 27.6 us)
Async XLA Ops:
  7.2 335.3 %all-gather.7.cloned.1.call-start = ((), (), s32[]{:S(2)}) async-start(), calls=%async_computation.12 | async-start | bytes 7864320 | tf_op jit(solution)/shard_map/all_gather | solution.py:32
  85.5 266.7 %all-gather.9.cloned.1.call-start = ((), (), s32[]{:S(2)}) async-start(), calls=%async_computation.13 | async-start | bytes 7864320 | tf_op jit(solution)/shard_map/all_gather | solution.py:32
  163.3 2.1 copy-start.2
  165.3 1.4 copy-start.5
  165.3 197.4 %all-gather.11.cloned.1.call-start = ((), (), s32[]{:S(2)}) async-start(), calls=%async_computation.14 | async-start | bytes 7864320 | tf_op jit(solution)/shard_map/all_gather | solution.py:66
  166.7 235.3 %all-gather.13.cloned.1.call-start = ((), (), s32[]{:S(2)}) async-start(), calls=%async_computation.15 | async-start | bytes 7864320 | tf_op jit(solution)/shard_map/all_gather | solution.py:32
  269.1 141.9 %all-gather.15.cloned.1.call-start = ((), (), s32[]{:S(2)}) async-start(), calls=%async_computation.16 | async-start | bytes 7864320 | tf_op jit(solution)/shard_map/all_gather | solution.py:32
  337.2 2.1 copy-start.3
  339.2 93.0 %all-gather.17.cloned.1.call-start = ((), (), s32[]{:S(2)}) async-start(), calls=%async_computation.17 | async-start | bytes 7864320 | tf_op jit(solution)/shard_map/all_gather | solution.py:69
  340.6 1.2 copy-start
  352.2 9.2 %copy-start.1 = (bf16[8,384,1024]{2,1,0:T(8,128)(2,1)S(1)}, bf16[8,384,1024]{2,1,0:T(8,128)(2,1)}, u32[]{:S(2)}) copy-start(bf16[8,384,1024]{2,1,0:T(8,128)(2,1)} %copy.49) | copy-start | bytes 18874372
  397.0 4.9 copy-start.4
  398.2 27.7 %all-to-all-start.5 = ((bf16[8,160,384]{2,1,0:T(8,128)(2,1)}), bf16[8,160,384]{2,1,0:T(8,128)(2,1)S(1)}, u32[]{:S(2)}, u32[]{:S(2)}) async-start(bf16[8,160,384]{2,1,0:T(8,128)(2,1)} %stack.4), calls=%async_computation.5 | async-start | bytes 1966080 | tf_op jit(solution)/shard_map/all_to_all | solution.py:22
  425.9 2.4 slice-start
  426.3 2.7 slice-start.1
  470.8 27.8 %all-to-all-start.11 = ((bf16[8,160,384]{2,1,0:T(8,128)(2,1)}), bf16[8,160,384]{2,1,0:T(8,128)(2,1)S(1)}, u32[]{:S(2)}, u32[]{:S(2)}) async-start(bf16[8,160,384]{2,1,0:T(8,128)(2,1)} %stack.5), calls=%async_computation.11 | async-start | bytes 1966080 | tf_op jit(solution)/shard_map/all_to_all | solution.py:22
  498.6 2.7 slice-start.2
  498.9 2.8 slice-start.3
  499.9 5.1 slice-start.4
  501.8 4.6 slice-start.5
Sparse Core Ops, SparseCore 0:
  85.6 57.7 all-gather.6
  165.4 61.2 all-gather.8
  228.8 46.1 all-gather.10
  276.5 50.5 all-gather.12
  339.3 44.4 all-gather.14
  385.8 46.3 all-gather.16
